TPU v7x, 32 devices: a whole 2x2x4 slice. The times are simulated.
32 devices in a mesh: ep: 16 (over z, y, core), tp: 2 (over x).
Axes of the slice: x: 2, y: 2, z: 4, core: 2. Of those that a mesh axis runs over, the one named last changes fastest.
Arguments:
- tokens: bfloat16 [128, 1024], P(('ep', 'tp')), may hold values from -6 to 6
- lengths: int32 [128], P('ep'), may hold values from 256 to 1024
- key_cache: bfloat16 [128, 1024, 128], P(('ep', 'tp')), may hold values from -1500 to 1500
- value_cache: bfloat16 [128, 1024, 128], P(('ep', 'tp')), may hold values from -6 to 6
- query_weight: bfloat16 [1024, 512], P(None, 'tp'), may hold values from -0.1875 to 0.1875
- key_weight: bfloat16 [1024, 128], replicated, may hold values from -0.1875 to 0.1875
- value_weight: bfloat16 [1024, 128], replicated, may hold values from -0.1875 to 0.1875
- lambdas: float32 [4], replicated, may hold values from 0.3 to 0.8
- head_gain: float32 [128], replicated, may hold values from 0.1 to 1.9
- output_weight: bfloat16 [512, 1024], P(None, 'tp'), may hold values from -0.25 to 0.25
- norm1_gain: float32 [1024], replicated, may hold values from 0.1 to 1.9
- routes: int32 [128, 6], P('ep'), may hold values from 0 to 15, all different within a row; in each aligned block of 8 rows (0 to 7, 8 to 15, ...) at most 6 rows name the same one
- route_logits: float32 [128, 6], P('ep'), may hold values from -9 to 410
- gate_weight: bfloat16 [16, 1024, 1024], P('ep', None, 'tp'), may hold values from -0.5 to 0.5
- up_weight: bfloat16 [16, 1024, 1024], P('ep', None, 'tp'), may hold values from -0.5 to 0.5
- down_weight: bfloat16 [16, 1024, 1024], P('ep', 'tp'), may hold values from -0.09375 to 0.09375
- norm2_gain: float32 [1024], replicated, may hold values from 0.1 to 1.9
Outputs:
- mixed: bfloat16 [128, 1024], P('ep', 'tp')
Inputs may be any that keep to these rules, and one draw needn't show every extreme that they name: `routes`: in the 8 rows of each aligned block (the rows held by one index of ep) no expert is named by more than 6 rows, a bound that some block reaches; the experts of a row differ.
All inputs are finite; a program needn't handle non-finite values.
Results may differ from a plain program's by a relative error of at most 0.014.
Values may be sent and summed in bfloat16 or wider, within the bound.
A program may use at most 64 MiB of HBM per device.

v0:
```python
import jax
import jax.numpy as jnp
from jax import lax
from jax.sharding import PartitionSpec as P

ALPHA = 1.4142135623730951
EPS = 1e-05
THETA = 500000.0
LIMIT = 7.0
SLOPE = 1.702


def rotate(values, positions):
    half = values.shape[-1] // 2
    freqs = THETA ** (-jnp.arange(half, dtype=jnp.float32) / half)
    angles = positions.astype(jnp.float32)[:, None] * freqs[None, :]
    shape = (angles.shape[0],) + (1,) * (values.ndim - 2) + (half,)
    cosine = jnp.cos(angles).reshape(shape)
    sine = jnp.sin(angles).reshape(shape)
    first = values[..., :half]
    second = values[..., half:]
    return jnp.concatenate(
        [first * cosine - second * sine, second * cosine + first * sine], axis=-1
    )


def scaled_part(summed, sums, squares, width, gain):
    mean = sums / width
    spread = squares / width - mean * mean
    return (summed - mean[:, None]) * lax.rsqrt(spread + EPS)[:, None] * gain


def choose_slots(routes_block, experts, capacity):
    flat = routes_block.reshape(-1)
    onehot = (flat[:, None] == jnp.arange(experts, dtype=jnp.int32)[None, :]).astype(jnp.int32)
    before = jnp.cumsum(onehot, axis=0) - onehot
    slot = jnp.sum(before * onehot, axis=1)
    target = flat * capacity + slot
    return target[:, None] == jnp.arange(experts * capacity, dtype=jnp.int32)[None, :]


def body(
    tokens,
    lengths,
    key_cache,
    value_cache,
    query_weight,
    key_weight,
    value_weight,
    lambdas,
    head_gain,
    output_weight,
    norm1_gain,
    routes,
    route_logits,
    gate_weight,
    up_weight,
    down_weight,
    norm2_gain,
):
    bf16 = jnp.bfloat16
    f32 = jnp.float32
    tp_count = lax.axis_size("tp")
    tp_rank = lax.axis_index("tp")
    own, width = tokens.shape
    group = own * tp_count
    part = width // tp_count
    heads = lambdas.shape[0]
    head_dim = key_weight.shape[1] // 2
    length = key_cache.shape[1]
    group_rows = lax.all_gather(tokens, "tp", axis=0, tiled=True)
    query = jnp.dot(group_rows, query_weight, preferred_element_type=f32).reshape(
        group, -1, 2, head_dim
    )
    query = rotate(query, lengths).astype(bf16).reshape(group, -1)
    query = lax.all_to_all(query, "tp", split_axis=0, concat_axis=1, tiled=True).reshape(
        own, heads, 2, head_dim
    )
    own_lengths = lax.dynamic_slice_in_dim(lengths, tp_rank * own, own)
    new_key = jnp.dot(tokens, key_weight, preferred_element_type=f32).reshape(own, 2, head_dim)
    new_key = rotate(new_key, own_lengths).astype(bf16)
    new_value = jnp.dot(tokens, value_weight, preferred_element_type=f32).astype(bf16)
    keys = key_cache.reshape(own, length, 2, head_dim)
    scale = head_dim ** (-0.5)
    past = jnp.einsum("bhmd,bjmd->bhmj", query, keys, preferred_element_type=f32) * scale
    live = jnp.arange(length, dtype=jnp.int32)[None, :] < own_lengths[:, None]
    past = jnp.where(live[:, None, None, :], past, -jnp.inf)
    selfs = jnp.einsum("bhmd,bmd->bhm", query, new_key, preferred_element_type=f32) * scale
    top = jnp.maximum(jnp.max(past, axis=-1), selfs)
    past_exp = jnp.exp(past - top[..., None])
    self_exp = jnp.exp(selfs - top)
    total = jnp.sum(past_exp, axis=-1) + self_exp
    past_prob = past_exp / total[..., None]
    self_prob = self_exp / total
    mixing = lambdas[None, :]
    past_weight = (past_prob[:, :, 0] - mixing[..., None] * past_prob[:, :, 1]).astype(bf16)
    self_weight = (self_prob[:, :, 0] - mixing * self_prob[:, :, 1]).astype(bf16)
    head_out = jnp.einsum("bhj,bje->bhe", past_weight, value_cache, preferred_element_type=f32)
    head_out = head_out + self_weight.astype(f32)[..., None] * new_value.astype(f32)[:, None, :]
    normed = (
        head_out
        * lax.rsqrt(jnp.mean(head_out * head_out, axis=-1, keepdims=True) + EPS)
        * head_gain
    )
    attended = normed.astype(bf16).reshape(own, -1)
    mix = jnp.dot(
        lax.all_gather(attended, "tp", axis=0, tiled=True),
        output_weight,
        preferred_element_type=f32,
    )
    column_start = tp_rank * part
    own_columns = lax.dynamic_slice_in_dim(group_rows, column_start, part, 1).astype(f32)
    summed = ALPHA * own_columns + mix
    sums, squares = lax.psum((jnp.sum(summed, axis=1), jnp.sum(summed * summed, axis=1)), "tp")
    gain_part = lax.dynamic_slice_in_dim(norm1_gain, column_start, part)
    settled_part = scaled_part(summed, sums, squares, width, gain_part).astype(bf16)
    settled = lax.all_gather(settled_part, "tp", axis=1, tiled=True)
    experts = lax.axis_size("ep")
    topk = routes.shape[1]
    capacity = min(group, max(2, 2 * group * topk // experts))
    chosen = choose_slots(routes, experts, capacity)
    placing = jnp.sum(chosen.reshape(group, topk, -1).astype(f32), axis=1).astype(bf16)
    route_weight = jax.nn.softmax(route_logits, axis=-1)
    gate_local = gate_weight[0]
    up_local = up_weight[0]
    down_local = down_weight[0]
    outgoing = lax.dot_general(
        placing, settled, (((0,), (0,)), ((), ())), preferred_element_type=f32
    )
    outgoing = outgoing.astype(bf16).reshape(experts, capacity, width)
    rows = lax.all_to_all(outgoing, "ep", split_axis=0, concat_axis=0, tiled=True)
    gate_h = jnp.einsum("scd,df->scf", rows, gate_local, preferred_element_type=f32)
    up_h = jnp.einsum("scd,df->scf", rows, up_local, preferred_element_type=f32)
    clipped = jnp.minimum(gate_h, LIMIT)
    linear = jnp.clip(up_h, -LIMIT, LIMIT)
    act = (clipped * jax.nn.sigmoid(SLOPE * clipped) * (linear + 1.0)).astype(bf16)
    terms = jnp.einsum("scf,fd->scd", act, down_local, preferred_element_type=f32)
    answers = (
        lax.psum_scatter(terms.astype(jnp.bfloat16), "tp", scatter_dimension=2, tiled=True)
        .astype(jnp.float32)
        .astype(bf16)
    )
    selector = chosen.astype(bf16)
    back = lax.all_to_all(answers, "ep", split_axis=0, concat_axis=0, tiled=True)
    picked = jnp.dot(selector, back.reshape(experts * capacity, -1), preferred_element_type=f32)
    routed = jnp.sum(picked.reshape(group, topk, -1) * route_weight[:, :, None], axis=1)
    final = ALPHA * settled_part.astype(f32) + routed
    sums, squares = lax.psum((jnp.sum(final, axis=1), jnp.sum(final * final, axis=1)), "tp")
    gain_part = lax.dynamic_slice_in_dim(norm2_gain, column_start, part)
    result = scaled_part(final, sums, squares, width, gain_part).astype(bf16)
    return result


def solution(mesh):
    in_specs = (
        P(("ep", "tp"), None),
        P("ep"),
        P(("ep", "tp"), None, None),
        P(("ep", "tp"), None, None),
        P(None, "tp"),
        P(),
        P(),
        P(),
        P(),
        P(None, "tp"),
        P(),
        P("ep", None),
        P("ep", None),
        P("ep", None, "tp"),
        P("ep", None, "tp"),
        P("ep", "tp", None),
        P(),
    )
    out_specs = P("ep", "tp")
    return jax.shard_map(body, mesh=mesh, in_specs=in_specs, out_specs=out_specs, check_vma=False)
```

profile of v0, /device:TPU:0, one launch (start us, length us, event | category | flops | bytes accessed | tf_op | source)
XLA Modules:
  0.0 96.1 jit_solution(3601989085853479555)
XLA Ops:
  6.6 0.7 copy-done.11
  7.3 5.6 %all-gather = bf16[2,4,1024]{2,1,0:T(4,128)(2,1)S(1)} all-gather(bf16[1,4,1024]{2,1,0:T(4,128)(2,1)} %bitcast.75), channel_id=1, replica_groups=mesh['ep'=16,'tp'=2] {'tp'}, dimensions={0}, use_global_device_ids=true | all-gather | bytes 24576 | tf_op jit(solution)/shard_map/all_gather | solution.py:71
  12.9 1.2 %fusion.54 = f32[8,256]{1,0:T(8,128)S(1)} fusion(bf16[8,1024]{1,0:T(8,128)(2,1)S(1)} %reshape.226, bf16[1024,256]{1,0:T(8,128)(2,1)} %param.21), kind=kOutput, calls=%fused_computation.97 | convolution fusion | flops 4194304 | bytes 548864 | tf_op jit(solution)/shard_map/dot_general | solution.py:72
  14.5 0.7 convert_element_type.66
  15.1 3.2 %all-to-all-start = ((bf16[2,4,256]{2,1,0:T(4,128)(2,1)}), bf16[2,4,256]{2,1,0:T(4,128)(2,1)S(1)}, u32[]{:S(2)}, u32[]{:S(2)}) async-start(bf16[2,4,256]{2,1,0:T(4,128)(2,1)} %convert_element_type.66), calls=%async_computation | async-start | bytes 8192 | tf_op jit(solution)/shard_map/all_to_all | solution.py:76
  18.6 1.1 %fusion.55 = f32[4,128]{1,0:T(4,128)S(1)} fusion(bf16[4,1024]{1,0:T(4,128)(2,1)} %param.17, bf16[1024,128]{1,0:T(8,128)(2,1)} %param.22), kind=kOutput, calls=%fused_computation.98 | convolution fusion | flops 1048576 | bytes 272384 | tf_op jit(solution)/shard_map/dot_general | solution.py:80
  19.9 0.8 fusion.6
  21.6 0.5 copy.54
  22.6 0.3 fusion.53
  23.3 0.6 copy-done.8
  24.0 0.4 multiply_reduce_fusion.2
  24.7 4.3 %all-gather.1 = bf16[2,4,512]{2,1,0:T(4,128)(2,1)S(1)} all-gather(bf16[1,4,512]{2,1,0:T(4,128)(2,1)S(1)} %reshape.227), channel_id=1, replica_groups=mesh['ep'=16,'tp'=2] {'tp'}, dimensions={0}, use_global_device_ids=true | all-gather | bytes 12288 | tf_op jit(solution)/shard_map/all_gather | solution.py:107
  29.4 4.9 %all-reduce.1 = (f32[8]{0:T(128)S(1)}, f32[8]{0:T(128)S(1)}) all-reduce(f32[8]{0:T(128)S(1)} %get-tuple-element.8, f32[8]{0:T(128)S(1)} %get-tuple-element.7), channel_id=1, replica_groups=mesh['ep'=16,'tp'=2] {'tp'}, use_global_device_ids=true, to_apply=%region_6.7 | all-reduce | flops 16 | bytes 128 | tf_op jit(solution)/shard_map/psum | solution.py:114
  34.4 4.4 %all_gather.11 = bf16[8,1024]{1,0:T(8,128)(2,1)S(1)} all-gather(bf16[8,512]{1,0:T(8,128)(2,1)S(1)} %multiply_convert_fusion.1), channel_id=1, replica_groups=mesh['ep'=16,'tp'=2] {'tp'}, dimensions={1}, use_global_device_ids=true | all-gather | bytes 24576 | tf_op jit(solution)/shard_map/all_gather | solution.py:117
  39.1 16.2 %all_to_all.23 = bf16[16,6,1024]{2,1,0:T(8,128)(2,1)S(1)} all-to-all(bf16[16,6,1024]{2,1,0:T(8,128)(2,1)S(1)} %reshape.222), channel_id=1, replica_groups=mesh['ep'=16,'tp'=2] {'ep'}, dimensions={0} | all-to-all | bytes 393216 | tf_op jit(solution)/shard_map/all_to_all | solution.py:131
  55.7 2.5 %convolution_convert_fusion = bf16[16,6,1024]{2,0,1:T(8,128)(2,1)} fusion(bf16[1,512,1024]{2,1,0:T(8,128)(2,1)S(1)} %copy-done, bf16[1,1024,512]{2,1,0:T(8,128)(2,1)} %param.31, f32[16,6,512]{2,0,1:T(8,128)S(1)} %convolution_minimum_fusion, bf16[16,6,1024]{2,1,0:T(8,128)(2,1)S(1)} %all_to_all.23), kind=kOutput, calls=%fused_computation | convolution fusion | flops 201867264 | bytes 2686976 | tf_op jit(solution)/shard_map/scf,fd->scd/dot_general | solution.py:137
  58.2 0.7 copy-done.6
  59.2 8.9 %reduce-scatter.2.cloned.1.call-done = bf16[16,6,512]{2,0,1:T(8,128)(2,1)} async-done(((bf16[16,6,1024]{2,0,1:T(8,128)(2,1)}), bf16[16,6,512]{2,0,1:T(8,128)(2,1)}) %reduce-scatter.2.cloned.1.call-update) | async-done | bytes 98320 | tf_op jit(solution)/shard_map/reduce_scatter | solution.py:139
  68.0 1.6 %copy.61 = bf16[16,6,512]{2,1,0:T(8,128)(2,1)} copy(bf16[16,6,512]{2,0,1:T(8,128)(2,1)} %reduce-scatter.2.cloned.1.call-done) | data formatting | bytes 196608 | tf_op jit(solution)/shard_map/reduce_scatter | solution.py:139
  69.6 5.6 %all-to-all-start.2 = ((bf16[16,6,512]{2,1,0:T(8,128)(2,1)}), bf16[16,6,512]{2,1,0:T(8,128)(2,1)S(1)}, u32[]{:S(2)}, u32[]{:S(2)}) async-start(bf16[16,6,512]{2,1,0:T(8,128)(2,1)} %copy.61), calls=%async_computation.3 | async-start | bytes 262144 | tf_op jit(solution)/shard_map/all_to_all | solution.py:144
  75.4 0.6 copy-done.10
  76.1 7.1 %all-to-all-done.2 = bf16[16,6,512]{2,1,0:T(8,128)(2,1)S(1)} async-done(((bf16[16,6,512]{2,1,0:T(8,128)(2,1)}), bf16[16,6,512]{2,1,0:T(8,128)(2,1)S(1)}, u32[]{:S(2)}, u32[]{:S(2)}) %all-to-all-start.2) | async-done | bytes 98336 | tf_op jit(solution)/shard_map/all_to_all | solution.py:144
  83.6 4.9 %all-reduce = (f32[8]{0:T(128)S(1)}, f32[8]{0:T(128)S(1)}) all-reduce(f32[8]{0:T(128)S(1)} %get-tuple-element.6, f32[8]{0:T(128)S(1)} %get-tuple-element.5), channel_id=1, replica_groups=mesh['ep'=16,'tp'=2] {'tp'}, use_global_device_ids=true, to_apply=%region_17.18 | all-reduce | flops 16 | bytes 128 | tf_op jit(solution)/shard_map/psum | solution.py:148
  88.6 0.7 multiply_convert_fusion
  (74 shorter events, 4.9 us)
Async XLA Ops:
  6.5 49.2 %copy-start = (bf16[1,512,1024]{2,1,0:T(8,128)(2,1)S(1)}, bf16[1,512,1024]{2,1,0:T(8,128)(2,1)}, u32[]{:S(2)}) copy-start(bf16[1,512,1024]{2,1,0:T(8,128)(2,1)} %param.32) | copy-start | bytes 3145732
  6.5 0.7 copy-start.11
  6.5 13.4 %copy-start.5 = (bf16[1024,128]{1,0:T(8,128)(2,1)S(1)}, bf16[1024,128]{1,0:T(8,128)(2,1)}, u32[]{:S(2)}) copy-start(bf16[1024,128]{1,0:T(8,128)(2,1)} %param.23) | copy-start | bytes 786436
  6.5 15.1 %copy-start.1 = (bf16[4,1024,128]{2,1,0:T(8,128)(2,1)S(1)}, bf16[4,1024,128]{2,1,0:T(8,128)(2,1)}, u32[]{:S(2)}) copy-start(bf16[4,1024,128]{2,1,0:T(8,128)(2,1)} %param.19) | copy-start | bytes 3145732
  15.1 7.2 %all-to-all-start = ((bf16[2,4,256]{2,1,0:T(4,128)(2,1)}), bf16[2,4,256]{2,1,0:T(4,128)(2,1)S(1)}, u32[]{:S(2)}, u32[]{:S(2)}) async-start(bf16[2,4,256]{2,1,0:T(4,128)(2,1)} %convert_element_type.66), calls=%async_computation | async-start | bytes 8192 | tf_op jit(solution)/shard_map/all_to_all | solution.py:76
  18.4 49.7 %reduce-scatter.2.cloned.1.call-start = ((), (), s32[]{:S(2)}) async-start(), calls=%async_computation.4 | async-start | bytes 294912 | tf_op jit(solution)/shard_map/reduce_scatter | solution.py:139
  19.9 0.9 copy-start.7
  21.6 0.7 copy-start.9
  22.1 1.8 %copy-start.2 = (bf16[4,1024,128]{2,1,0:T(8,128)(2,1)S(1)}, bf16[4,1024,128]{2,1,0:T(8,128)(2,1)}, u32[]{:S(2)}) copy-start(bf16[4,1024,128]{2,1,0:T(8,128)(2,1)} %param.20) | copy-start | bytes 3145732
  23.3 0.7 copy-start.8
  24.0 0.7 copy-start.12
  24.0 5.1 %copy-start.4 = (bf16[512,512]{1,0:T(8,128)(2,1)S(1)}, bf16[512,512]{1,0:T(8,128)(2,1)}, u32[]{:S(2)}) copy-start(bf16[512,512]{1,0:T(8,128)(2,1)} %param.26) | copy-start | bytes 1572868
  24.4 31.0 %copy-start.3 = (bf16[1,1024,512]{2,1,0:T(8,128)(2,1)S(1)}, bf16[1,1024,512]{2,1,0:T(8,128)(2,1)}, u32[]{:S(2)}) copy-start(bf16[1,1024,512]{2,1,0:T(8,128)(2,1)} %param.30) | copy-start | bytes 3145732
  58.2 0.7 copy-start.6
  69.6 13.5 %all-to-all-start.2 = ((bf16[16,6,512]{2,1,0:T(8,128)(2,1)}), bf16[16,6,512]{2,1,0:T(8,128)(2,1)S(1)}, u32[]{:S(2)}, u32[]{:S(2)}) async-start(bf16[16,6,512]{2,1,0:T(8,128)(2,1)} %copy.61), calls=%async_computation.3 | async-start | bytes 262144 | tf_op jit(solution)/shard_map/all_to_all | solution.py:144
  75.3 0.7 copy-start.10
Sparse Core Ops, SparseCore 0:
  58.3 9.6 reduce-scatter.1
where the time goes:
time: 96.8 us; the launch traced here: 96.1 us
  blocking collectives  40.4 us (42%)
  waiting for transfers between devices  15.9 us (16%)
  between operations  13.6 us (14%)
  starting transfers between devices  8.9 us (9%)
  matrix products  7.6 us (8%)
  local copies, waits for them, and re-layouts  6.75 us (7%)
  other arithmetic  2.98 us (3%)
    all_to_all x1, blocking collectives, body(): lax.all_to_all(outgoing, 'ep', split_axis=0, concat_axis=0, tiled=True)  16.2 us
    reduce_scatter x1, waiting for transfers between devices, body(): lax.psum_scatter(terms.astype(jnp.bfloat16), 'tp', scatter_dimension=2, t...  8.86 us
    all_to_all x1, waiting for transfers between devices, body(): lax.all_to_all(answers, 'ep', split_axis=0, concat_axis=0, tiled=True)  7.06 us
    all_to_all x1, starting transfers between devices, body(): lax.all_to_all(answers, 'ep', split_axis=0, concat_axis=0, tiled=True)  5.63 us
    all_gather x1, blocking collectives, body(): group_rows = lax.all_gather(tokens, 'tp', axis=0, tiled=True)  5.56 us
    psum x1, blocking collectives, body(): lax.psum((jnp.sum(summed, axis=1), jnp.sum(summed * summed, axis=1)), 'tp')  4.93 us
    psum x1, blocking collectives, body(): lax.psum((jnp.sum(final, axis=1), jnp.sum(final * final, axis=1)), 'tp')  4.93 us
    all_gather x1, blocking collectives, body(): settled = lax.all_gather(settled_part, 'tp', axis=1, tiled=True)  4.35 us
  transfers between devices with their start and end apart: 3, of which 2 were waited for; matrix products, arithmetic and copies ran while one was open for 4% of the time, Pallas kernels for 0%

commit v1 on v0

v1 whole, which is shorter than its diff:
```python
import functools
import math

import jax
import jax.numpy as jnp
from jax import lax
from jax.experimental import pallas as pl
from jax.experimental.pallas import tpu as pltpu
from jax.sharding import PartitionSpec as P

ALPHA = 1.4142135623730951
EPS = 1e-05
THETA = 500000.0
LIMIT = 7.0
SLOPE = 1.702
LANES = 128
MESH = pl.DeviceIdType.MESH
BF16 = jnp.bfloat16
F32 = jnp.float32


def repeat(count, step):
    if count <= 32:
        for i in range(count):
            step(i)
    else:
        lax.fori_loop(0, count, lambda i, _: (step(i), 0)[1], 0)


def column(values, rows):
    row = lax.broadcasted_iota(jnp.int32, (rows, LANES), 0)
    out = jnp.zeros((rows, LANES), F32)
    for r, value in enumerate(values):
        out = jnp.where(row == r, value, out)
    return out


def turns(positions, head_dim):
    half = head_dim // 2
    lane = lax.broadcasted_iota(jnp.int32, positions.shape, 1)
    index = lane % half
    freq = jnp.ones(positions.shape, F32)
    for bit in range(half.bit_length() - 1):
        factor = THETA ** (-(1 << bit) / half)
        freq = jnp.where((index // (1 << bit)) % 2 == 1, freq * factor, freq)
    angle = positions * freq
    sine = jnp.sin(angle)
    return jnp.cos(angle), jnp.where(lane % head_dim < half, -sine, sine)


def turn(values, cosine, sine, head_dim):
    half = head_dim // 2
    lane = lax.broadcasted_iota(jnp.int32, values.shape, 1)
    ahead = pltpu.roll(values, LANES - half, 1)
    behind = pltpu.roll(values, half, 1)
    other = jnp.where(lane % head_dim < half, ahead, behind)
    return values * cosine + other * sine


def kernel(
    n_ep, n_tp, head_dim,
    tokens_h, lengths_h, kc_h, vc_h, qw_h, kw_h, vw_h, lambdas_h, hg_h, ow_h, g1_h,
    routes_h, logits_h, gw_h, uw_h, dw_h, g2_h,
    out_ref,
    tok, lens, kc, vc, qw, kw, vw, lam, hg, ow, g1, routes, logits, gw, uw, dw, g2,
    tokf, qsend, qrecv, att, sm, blocks, wall, zs, zr, zm, rs, rr, st,
    in_sem, tok_s, tok_r, q_s, q_r, att_s, att_r, w_s, w_r,
    b_s, b_r, f_s, f_r, z_s, z_r, r_s, r_r, st_s, st_r,
):
    e = lax.axis_index("ep")
    t = lax.axis_index("tp")
    core = lax.rem(e, 2)
    chip = e // 2
    other = 1 - core
    sibling = chip * 2 + other
    n_dev = n_ep * n_tp
    nh = n_ep // 2
    n_same = nh * n_tp
    own, width = tokens_h.shape
    group = own * n_tp
    part = width // n_tp
    heads = lambdas_h.shape[0]
    heads_here = heads // n_tp
    topk = routes_h.shape[1]
    length = kc_h.shape[1]
    flat = e * n_tp + t

    barrier = pltpu.get_barrier_semaphore()

    def greet(i):
        peer = lax.rem(flat + i + 1, n_dev)
        pl.semaphore_signal(
            barrier, inc=1, device_id=(peer // n_tp, lax.rem(peer, n_tp)), device_id_type=MESH
        )

    repeat(n_dev - 1, greet)

    pairs = [
        (tokens_h, tok.at[t]), (lengths_h, lens), (routes_h, routes), (logits_h, logits),
        (kw_h, kw), (vw_h, vw), (qw_h, qw), (lambdas_h, lam), (hg_h, hg), (g1_h, g1), (g2_h, g2),
        (kc_h, kc), (vc_h, vc), (ow_h, ow), (gw_h.at[0], gw), (uw_h.at[0], uw), (dw_h.at[0], dw),
    ]
    loads = [pltpu.make_async_copy(a, b, in_sem.at[i]) for i, (a, b) in enumerate(pairs)]
    for load in loads:
        load.start()
    (l_tok, l_len, l_routes, l_logits, l_kw, l_vw, l_qw, l_lam, l_hg, l_g1, l_g2,
     l_kc, l_vc, l_ow, l_gw, l_uw, l_dw) = loads

    l_routes.wait()
    l_logits.wait()
    raw = logits[...]
    grown = jnp.exp(raw - jnp.max(raw, axis=1, keepdims=True))
    share = grown / jnp.sum(grown, axis=1, keepdims=True)
    named = routes[...]
    lanes = wall.shape[2]
    lane_w = lax.broadcasted_iota(jnp.int32, (group, lanes), 1)
    dense = jnp.zeros((group, lanes), F32)
    for k in range(topk):
        dense = jnp.where(named[:, k:k + 1] == lane_w, share[:, k:k + 1], dense)
    my_slot = core * nh + chip
    wall[my_slot] = dense

    l_len.wait()
    cos_g, sin_g = turns(column([lens[r].astype(F32) for r in range(group)], group), head_dim)
    own_lens = [lens[t * own + r] for r in range(own)]
    cos_o, sin_o = turns(column([v.astype(F32) for v in own_lens], own), head_dim)

    l_tok.wait()
    pl.semaphore_wait(barrier, n_dev - 1)

    def swap(ref, send, recv, src_of=None):
        copies = []
        for d in range(1, n_tp):
            to = lax.rem(t + d, n_tp)
            src = ref.at[t] if src_of is None else src_of.at[to]
            copies.append(pltpu.make_async_remote_copy(
                src_ref=src, dst_ref=ref.at[t], send_sem=send.at[d - 1], recv_sem=recv.at[d - 1],
                device_id=(e, to), device_id_type=MESH,
            ))
        for copy in copies:
            copy.start()
        return copies

    tok_copies = swap(tok, tok_s, tok_r)

    def send_w(i):
        to = lax.rem(e + i + 1, n_ep)
        pltpu.make_async_remote_copy(
            src_ref=wall.at[my_slot], dst_ref=wall.at[my_slot], send_sem=w_s, recv_sem=w_r,
            device_id=(to, t), device_id_type=MESH,
        ).start()

    repeat(n_ep - 1, send_w)

    mine = tok[t]
    l_kw.wait()
    new_key = jnp.dot(mine, kw[...], preferred_element_type=F32)
    new_key = turn(new_key, cos_o, sin_o, head_dim).astype(BF16).astype(F32)
    l_vw.wait()
    new_value = jnp.dot(mine, vw[...], preferred_element_type=F32).astype(BF16).astype(F32)

    l_qw.wait()
    for copy in tok_copies:
        copy.wait_recv()
    for s in range(n_tp):
        tokf[s * own:(s + 1) * own, :] = tok[s].astype(F32)
    query = jnp.dot(tokf[...].astype(BF16), qw[...], preferred_element_type=F32)
    for h in range(heads_here):
        cut = slice(h * LANES, (h + 1) * LANES)
        turned = turn(query[:, cut], cos_g, sin_g, head_dim)
        for s in range(n_tp):
            qsend[s, :, cut] = turned[s * own:(s + 1) * own, :].astype(BF16)
    q_copies = swap(qrecv, q_s, q_r, qsend)
    qrecv[t] = qsend[t]

    l_lam.wait()
    l_hg.wait()
    l_kc.wait()
    l_vc.wait()
    for copy in q_copies:
        copy.wait_recv()

    scale = head_dim ** (-0.5)
    rows2 = 2 * heads
    row = lax.broadcasted_iota(jnp.int32, (rows2, LANES), 0)
    lane = lax.broadcasted_iota(jnp.int32, (rows2, LANES), 1)
    my_map = (row // heads) == (lane // head_dim)
    position = lax.broadcasted_iota(jnp.int32, (rows2, length), 1)
    mixing = column([lam[h] for h in range(heads)], heads)[:, :1]
    queries = [qrecv[s].astype(F32) for s in range(n_tp)]
    outs = []
    for b in range(own):
        qm = jnp.zeros((rows2, LANES), F32)
        for h in range(heads):
            at = (h % heads_here) * LANES
            piece = queries[h // heads_here][b:b + 1, at:at + LANES]
            qm = jnp.where(row % heads == h, piece, qm)
        qm = jnp.where(my_map, qm, 0.0)
        past = lax.dot_general(
            qm.astype(BF16), kc[b], (((1,), (1,)), ((), ())), preferred_element_type=F32
        ) * scale
        past = jnp.where(position < own_lens[b], past, -jnp.inf)
        selfs = jnp.sum(qm * new_key[b:b + 1, :], axis=1, keepdims=True) * scale
        top = jnp.maximum(jnp.max(past, axis=1, keepdims=True), selfs)
        past_exp = jnp.exp(past - top)
        self_exp = jnp.exp(selfs - top)
        total = jnp.sum(past_exp, axis=1, keepdims=True) + self_exp
        past_prob = past_exp / total
        self_prob = self_exp / total
        weight = (past_prob[:heads] - mixing * past_prob[heads:]).astype(BF16)
        self_weight = (self_prob[:heads] - mixing * self_prob[heads:]).astype(BF16).astype(F32)
        head_out = jnp.dot(weight, vc[b], preferred_element_type=F32)
        head_out = head_out + self_weight * new_value[b:b + 1, :]
        square = jnp.mean(head_out * head_out, axis=1, keepdims=True)
        outs.append(head_out * lax.rsqrt(square + EPS) * hg[...])
    row_o = lax.broadcasted_iota(jnp.int32, (own, LANES), 0)
    for h in range(heads):
        piece = jnp.zeros((own, LANES), F32)
        for b in range(own):
            piece = jnp.where(row_o == b, outs[b][h:h + 1, :], piece)
        att[t, :, h * LANES:(h + 1) * LANES] = piece.astype(BF16)
    att_copies = swap(att, att_s, att_r)

    l_ow.wait()
    l_g1.wait()
    l_g2.wait()
    cols = pl.ds(pl.multiple_of(t * part, LANES), part)
    for copy in att_copies:
        copy.wait_recv()
    for s in range(n_tp):
        sm[s * own:(s + 1) * own, :] = att[s].astype(F32)
    mix = jnp.dot(sm[...].astype(BF16), ow[...], preferred_element_type=F32)
    summed = ALPHA * tokf[:, cols] + mix
    blocks[core, t, chip] = summed.astype(BF16)

    rank = chip * n_tp + t

    def send_block(i):
        to = lax.rem(rank + i + 1, n_same)
        pltpu.make_async_remote_copy(
            src_ref=blocks.at[core, t, chip], dst_ref=blocks.at[core, t, chip],
            send_sem=b_s, recv_sem=b_r.at[i],
            device_id=(to // n_tp * 2 + core, lax.rem(to, n_tp)), device_id_type=MESH,
        ).start()

    repeat(n_same - 1, send_block)

    def forward(src):
        at = blocks.at[core, lax.rem(src, n_tp), src // n_tp]
        pltpu.make_async_remote_copy(
            src_ref=at, dst_ref=at, send_sem=f_s, recv_sem=f_r,
            device_id=(sibling, t), device_id_type=MESH,
        ).start()

    forward(rank)

    def take_block(i):
        src = lax.rem(rank - (i + 1) + n_same, n_same)
        at = blocks.at[core, lax.rem(src, n_tp), src // n_tp]
        pltpu.make_async_remote_copy(
            src_ref=at, dst_ref=at, send_sem=b_s, recv_sem=b_r.at[i],
            device_id=(sibling, t), device_id_type=MESH,
        ).wait_recv()
        forward(src)

    repeat(n_same - 1, take_block)

    def await_bytes(ref, sem):
        pltpu.make_async_copy(ref, ref, sem).wait()

    await_bytes(wall.at[pl.ds(0, n_ep - 1)], w_r)
    l_gw.wait()
    l_uw.wait()
    l_dw.wait()

    count = max(1, min(nh, 128 // group))
    rows = count * group

    def settle(pieces, gains):
        mean = sum(jnp.sum(x, axis=-1, keepdims=True) for x in pieces) / width
        pieces = [x - mean for x in pieces]
        spread = sum(jnp.sum(x * x, axis=-1, keepdims=True) for x in pieces) / width
        inverse = lax.rsqrt(spread + EPS)
        return [x * inverse * g for x, g in zip(pieces, gains)]

    gains = [g1[:, s * part:(s + 1) * part] for s in range(n_tp)]

    def expert(parity, store):
        def step(c):
            first = c * count
            pieces = [
                blocks[parity, s, pl.ds(first, count)].astype(F32).reshape(rows, part)
                for s in range(n_tp)
            ]
            x = jnp.concatenate([v.astype(BF16) for v in settle(pieces, gains)], axis=1)
            gate = jnp.dot(x, gw[...], preferred_element_type=F32)
            up = jnp.dot(x, uw[...], preferred_element_type=F32)
            clipped = jnp.minimum(gate, LIMIT)
            linear = jnp.clip(up, -LIMIT, LIMIT)
            act = (clipped * jax.nn.sigmoid(SLOPE * clipped) * (linear + 1.0)).astype(BF16)
            dense = wall[pl.ds(parity * nh + first, count)].reshape(rows, lanes)
            lane_e = lax.broadcasted_iota(jnp.int32, dense.shape, 1)
            share = jnp.sum(jnp.where(lane_e == e, dense, 0.0), axis=1, keepdims=True)
            terms = jnp.dot(act, dw[...], preferred_element_type=F32) * share
            for s in range(n_tp):
                store(s, first, terms[:, s * part:(s + 1) * part].reshape(count, group, part))

        repeat(nh // count, step)

    def store_sibling(s, first, value):
        zs[s, pl.ds(first, count)] = value.astype(BF16)

    def store_mine(s, first, value):
        zm[s, pl.ds(first, count)] = value

    expert(core, store_sibling)
    z_copy = pltpu.make_async_remote_copy(
        src_ref=zs, dst_ref=zr, send_sem=z_s, recv_sem=z_r,
        device_id=(sibling, t), device_id_type=MESH,
    )
    z_copy.start()
    await_bytes(blocks.at[other], f_r)
    expert(other, store_mine)
    z_copy.wait_recv()

    def add_chunk(c):
        at = pl.ds(c * count, count)
        for s in range(n_tp):
            rs[s, at] = (zm[s, at] + zr[s, at].astype(F32)).astype(BF16)

    repeat(nh // count, add_chunk)

    def send_result(i):
        to = lax.rem(rank + i, n_same)
        to_chip = to // n_tp
        to_tp = lax.rem(to, n_tp)
        pltpu.make_async_remote_copy(
            src_ref=rs.at[to_tp, to_chip], dst_ref=rr.at[t, chip], send_sem=r_s, recv_sem=r_r,
            device_id=(to_chip * 2 + other, to_tp), device_id_type=MESH,
        ).start()

    repeat(n_same, send_result)

    pieces = [blocks[core, s, chip].astype(F32) for s in range(n_tp)]
    mean = sum(jnp.sum(x, axis=1, keepdims=True) for x in pieces) / width
    spread = sum(jnp.sum((x - mean) * (x - mean), axis=1, keepdims=True) for x in pieces) / width
    here = blocks[core, t, chip].astype(F32)
    settled = ((here - mean) * lax.rsqrt(spread + EPS) * g1[:, cols]).astype(BF16).astype(F32)

    await_bytes(rr, r_r)
    final = ALPHA * settled
    if n_same <= 32:
        for s in range(n_tp):
            for c in range(nh):
                final = final + rr[s, c].astype(F32)
    else:
        def add(i, total):
            return total + rr[lax.rem(i, n_tp), i // n_tp].astype(F32)

        final = lax.fori_loop(0, n_same, add, final)
    lane_s = lax.broadcasted_iota(jnp.int32, (group, LANES), 1)
    sums = jnp.sum(final, axis=1, keepdims=True)
    squares = jnp.sum(final * final, axis=1, keepdims=True)
    st[t] = jnp.where(lane_s == 0, sums, squares)
    st_copies = swap(st, st_s, st_r)
    for copy in st_copies:
        copy.wait_recv()
    stats = sum(st[s] for s in range(n_tp)) / width
    mean = stats[:, 0:1]
    spread = stats[:, 1:2] - mean * mean
    out_ref[...] = ((final - mean) * lax.rsqrt(spread + EPS) * g2[:, cols]).astype(BF16)

    for copy in tok_copies + q_copies + att_copies + st_copies + [z_copy]:
        copy.wait_send()
    await_bytes(wall.at[pl.ds(0, n_ep - 1)], w_s)
    await_bytes(rr, r_s)
    await_bytes(blocks.at[core], f_s)
    if n_tp > 1:
        await_bytes(blocks.at[core, pl.ds(0, n_tp - 1)], b_s)
    await_bytes(blocks.at[core, 0, pl.ds(0, nh - 1)], b_s)


def body(mesh_shape, *args):
    (tokens, lengths, key_cache, value_cache, query_weight, key_weight, value_weight, lambdas,
     head_gain, output_weight, norm1_gain, routes, route_logits, gate_weight, up_weight,
     down_weight, norm2_gain) = args
    n_ep, n_tp = mesh_shape
    own, width = tokens.shape
    group = own * n_tp
    part = width // n_tp
    nh = n_ep // 2
    n_same = nh * n_tp
    heads = lambdas.shape[0]
    value_dim = value_weight.shape[1]
    head_dim = key_weight.shape[1] // 2
    lanes = -(-n_ep // LANES) * LANES
    operands = (
        tokens, lengths, key_cache, value_cache, query_weight, key_weight, value_weight, lambdas,
        head_gain.reshape(1, -1), output_weight, norm1_gain.reshape(1, -1), routes, route_logits,
        gate_weight, up_weight, down_weight, norm2_gain.reshape(1, -1),
    )
    v = pltpu.VMEM
    dma = pltpu.SemaphoreType.DMA
    partners = max(1, n_tp - 1)
    scratch = [
        v((n_tp, own, width), BF16), pltpu.SMEM(lengths.shape, jnp.int32),
        v(key_cache.shape, BF16), v(value_cache.shape, BF16), v(query_weight.shape, BF16),
        v(key_weight.shape, BF16), v(value_weight.shape, BF16), pltpu.SMEM(lambdas.shape, F32),
        v((1, value_dim), F32), v(output_weight.shape, BF16), v((1, width), F32),
        v(routes.shape, jnp.int32), v(route_logits.shape, F32), v(gate_weight.shape[1:], BF16),
        v(up_weight.shape[1:], BF16), v(down_weight.shape[1:], BF16), v((1, width), F32),
        v((group, width), F32),
        v((n_tp, own, query_weight.shape[1]), BF16), v((n_tp, own, query_weight.shape[1]), BF16),
        v((n_tp, own, heads * value_dim), BF16), v((group, heads * value_dim), F32),
        v((2, n_tp, nh, group, part), BF16), v((n_ep, group, lanes), F32),
        v((n_tp, nh, group, part), BF16), v((n_tp, nh, group, part), BF16),
        v((n_tp, nh, group, part), F32), v((n_tp, nh, group, part), BF16),
        v((n_tp, nh, group, part), BF16), v((n_tp, group, LANES), F32),
        dma((len(operands),)), dma((partners,)), dma((partners,)), dma((partners,)),
        dma((partners,)), dma((partners,)), dma((partners,)), dma, dma,
        dma, dma((n_same - 1,)), dma, dma, dma, dma, dma, dma, dma((partners,)), dma((partners,)),
    ]
    return pl.pallas_call(
        functools.partial(kernel, n_ep, n_tp, head_dim),
        out_shape=jax.ShapeDtypeStruct((group, part), BF16),
        in_specs=[pl.BlockSpec(memory_space=pl.ANY)] * len(operands),
        out_specs=pl.BlockSpec(memory_space=pltpu.VMEM),
        scratch_shapes=scratch,
        compiler_params=pltpu.CompilerParams(
            collective_id=0, has_side_effects=True, vmem_limit_bytes=60 * 1024 * 1024
        ),
    )(*operands)


def solution(mesh):
    in_specs = (
        P(("ep", "tp"), None),
        P("ep"),
        P(("ep", "tp"), None, None),
        P(("ep", "tp"), None, None),
        P(None, "tp"),
        P(),
        P(),
        P(),
        P(),
        P(None, "tp"),
        P(),
        P("ep", None),
        P("ep", None),
        P("ep", None, "tp"),
        P("ep", None, "tp"),
        P("ep", "tp", None),
        P(),
    )
    out_specs = P("ep", "tp")
    shape = (mesh.shape["ep"], mesh.shape["tp"])
    return jax.shard_map(
        functools.partial(body, shape), mesh=mesh, in_specs=in_specs, out_specs=out_specs,
        check_vma=False,
    )
```

time: 96.8 us -> 34 us (0.35)
  blocking collectives: 40.4 us -> 0 us
  Pallas kernels: 0 us -> 32.5 us
  waiting for transfers between devices: 15.9 us -> 0 us
  between operations: 13.6 us -> 0.01 us
  starting transfers between devices: 8.9 us -> 0 us
  matrix products: 7.6 us -> 0 us
  local copies, waits for them, and re-layouts: 6.75 us -> 1.3 us
  other arithmetic: 2.98 us -> 0 us
    pallas_call x0 -> x1, Pallas kernels: none -> 32.5 us  [body(): pl.pallas_call(functools.partial(kernel, n_ep, n_tp, head_dim), out_shape...]
    all_to_all x1 -> x0, blocking collectives: 16.2 us -> none  [body(): lax.all_to_all(outgoing, 'ep', split_axis=0, concat_axis=0, tiled=True)]
    all_gather x3 -> x0, blocking collectives: 14.3 us -> none  [the longest x1 5.56 us: body(): group_rows = lax.all_gather(tokens, 'tp', axis=0, tiled=True)]
    psum x2 -> x0, blocking collectives: 9.87 us -> none  [the longest x1 4.93 us: body(): lax.psum((jnp.sum(summed, axis=1), jnp.sum(summed * summed, axis=1)), 'tp')]
    reduce_scatter x1 -> x0, waiting for transfers between devices: 8.86 us -> none  [body(): lax.psum_scatter(terms.astype(jnp.bfloat16), 'tp', scatter_dimension=2, t...]
    all_to_all x2 -> x0, starting transfers between devices: 8.86 us -> none  [the longest x1 5.63 us: body(): lax.all_to_all(answers, 'ep', split_axis=0, concat_axis=0, tiled=True)]
    dot_general x11 -> x0, matrix products: 7.6 us -> none  [the longest x1 2.49 us: body(): jnp.einsum('scf,fd->scd', act, down_local, preferred_element_type=f32)]
    all_to_all x2 -> x0, waiting for transfers between devices: 7.06 us -> none  [the longest x1 7.06 us: body(): lax.all_to_all(answers, 'ep', split_axis=0, concat_axis=0, tiled=True)]
  transfers between devices with their start and end apart: 3 -> 0, of which waited for: 2 -> 0; matrix products, arithmetic and copies ran while one was open for 4% -> 0% of each run, Pallas kernels for 0% -> 0%
where the time goes in v1:
time: 34 us; the launch traced here: 33.8 us
  Pallas kernels  32.5 us (96%)
  local copies, waits for them, and re-layouts  1.3 us (4%)
    pallas_call x1, Pallas kernels, body(): pl.pallas_call(functools.partial(kernel, n_ep, n_tp, head_dim), out_shape...  32.5 us
    unnamed x1, local copies, waits for them, and re-layouts  1.3 us

profile of v1, /device:TPU:0, one launch (start us, length us, event | category | flops | bytes accessed | tf_op | source)
XLA Modules:
  0.0 33.8 jit_solution(561928120728208360)
XLA Ops:
  0.0 32.5 %shard_map.163 = bf16[8,512]{1,0:T(8,128)(2,1)} custom-call(bf16[4,1024]{1,0:T(4,128)(2,1)} %tokens_h.1, s32[8]{0:T(128)} %lengths_h.1, bf16[4,1024,128]{2,1,0:T(8,128)(2,1)} %kc_h.1, bf16[4,1024,128]{2,1,0:T(8,128)(2,1)} %vc_h.1, bf16[1024,256]{1,0:T(8,128)(2,1)} %qw_h.1, bf16[1024,128]{1,0:T(8,128)(2,1)} %kw_h.1, bf16[1024,128]{1,0:T(8,128)(2,1)} %vw_h.1, ...), custom_call_target="tpu_custom_call" | custom-call | tf_op jit(solution)/shard_map/pallas_call | solution.py:423
  32.5 1.3 %copy.19 = bf16[8,512]{1,0:T(8,128)(2,1)} copy(bf16[8,512]{1,0:T(8,128)(2,1)} %shard_map.163) | data formatting | bytes 16384

commit v2 on v1

--- a/solution.py
+++ b/solution.py
@@ -65,7 +65,7 @@
     tok, lens, kc, vc, qw, kw, vw, lam, hg, ow, g1, routes, logits, gw, uw, dw, g2,
     tokf, qsend, qrecv, att, sm, blocks, wall, zs, zr, zm, rs, rr, st,
     in_sem, tok_s, tok_r, q_s, q_r, att_s, att_r, w_s, w_r,
-    b_s, b_r, f_s, f_r, z_s, z_r, r_s, r_r, st_s, st_r,
+    b_s, b_r, f_s, f_r, z_s, z_r, r_s, r_r, st_s, st_r, round_s,
 ):
     e = lax.axis_index("ep")
     t = lax.axis_index("tp")
@@ -86,14 +86,19 @@
     flat = e * n_tp + t
 
     barrier = pltpu.get_barrier_semaphore()
-
-    def greet(i):
-        peer = lax.rem(flat + i + 1, n_dev)
-        pl.semaphore_signal(
-            barrier, inc=1, device_id=(peer // n_tp, lax.rem(peer, n_tp)), device_id_type=MESH
-        )
-
-    repeat(n_dev - 1, greet)
+    bits = (n_dev - 1).bit_length()
+
+    def across(k):
+        step = 1 << k
+        peer = flat + step * (1 - 2 * lax.rem(flat // step, 2))
+        return (peer // n_tp, lax.rem(peer, n_tp))
+
+    for k in range(bits):
+        pl.semaphore_signal(barrier, inc=1, device_id=across(k), device_id_type=MESH)
+
+    def spread(k):
+        pl.semaphore_signal(round_s.at[k], inc=1, device_id=across(k), device_id_type=MESH)
+        pl.semaphore_wait(round_s.at[k], 1)
 
     pairs = [
         (tokens_h, tok.at[t]), (lengths_h, lens), (routes_h, routes), (logits_h, logits),
@@ -126,7 +131,7 @@
     cos_o, sin_o = turns(column([v.astype(F32) for v in own_lens], own), head_dim)
 
     l_tok.wait()
-    pl.semaphore_wait(barrier, n_dev - 1)
+    pl.semaphore_wait(barrier, bits)
 
     def swap(ref, send, recv, src_of=None):
         copies = []
@@ -150,7 +155,6 @@
             device_id=(to, t), device_id_type=MESH,
         ).start()
 
-    repeat(n_ep - 1, send_w)
 
     mine = tok[t]
     l_kw.wait()
@@ -160,6 +164,8 @@
     new_value = jnp.dot(mine, vw[...], preferred_element_type=F32).astype(BF16).astype(F32)
 
     l_qw.wait()
+    for k in range(1, min(4, bits)):
+        spread(k)
     for copy in tok_copies:
         copy.wait_recv()
     for s in range(n_tp):
@@ -172,6 +178,9 @@
             qsend[s, :, cut] = turned[s * own:(s + 1) * own, :].astype(BF16)
     q_copies = swap(qrecv, q_s, q_r, qsend)
     qrecv[t] = qsend[t]
+    for k in range(4, bits):
+        spread(k)
+    repeat(n_ep - 1, send_w)
 
     l_lam.wait()
     l_hg.wait()
@@ -234,12 +243,14 @@
     blocks[core, t, chip] = summed.astype(BF16)
 
     rank = chip * n_tp + t
+    low = rank < n_same // 2
 
     def send_block(i):
-        to = lax.rem(rank + i + 1, n_same)
+        v = jnp.where(low, n_same - 2 - i, i)
+        to = v + (v >= rank).astype(jnp.int32)
         pltpu.make_async_remote_copy(
             src_ref=blocks.at[core, t, chip], dst_ref=blocks.at[core, t, chip],
-            send_sem=b_s, recv_sem=b_r.at[i],
+            send_sem=b_s, recv_sem=b_r.at[rank],
             device_id=(to // n_tp * 2 + core, lax.rem(to, n_tp)), device_id_type=MESH,
         ).start()
 
@@ -258,7 +269,7 @@
         src = lax.rem(rank - (i + 1) + n_same, n_same)
         at = blocks.at[core, lax.rem(src, n_tp), src // n_tp]
         pltpu.make_async_remote_copy(
-            src_ref=at, dst_ref=at, send_sem=b_s, recv_sem=b_r.at[i],
+            src_ref=at, dst_ref=at, send_sem=b_s, recv_sem=b_r.at[src],
             device_id=(sibling, t), device_id_type=MESH,
         ).wait_recv()
         forward(src)
@@ -331,7 +342,7 @@
     repeat(nh // count, add_chunk)
 
     def send_result(i):
-        to = lax.rem(rank + i, n_same)
+        to = jnp.where(low, n_same - 1 - i, i)
         to_chip = to // n_tp
         to_tp = lax.rem(to, n_tp)
         pltpu.make_async_remote_copy(
@@ -418,11 +429,12 @@
         v((n_tp, nh, group, part), BF16), v((n_tp, group, LANES), F32),
         dma((len(operands),)), dma((partners,)), dma((partners,)), dma((partners,)),
         dma((partners,)), dma((partners,)), dma((partners,)), dma, dma,
-        dma, dma((n_same - 1,)), dma, dma, dma, dma, dma, dma, dma((partners,)), dma((partners,)),
+        dma, dma((n_same,)), dma, dma, dma, dma, dma, dma, dma((partners,)), dma((partners,)),
+        pltpu.SemaphoreType.REGULAR(((n_ep * n_tp).bit_length(),)),
     ]
     return pl.pallas_call(
         functools.partial(kernel, n_ep, n_tp, head_dim),
-        out_shape=jax.ShapeDtypeStruct((group, part), BF16),
+        out_shape=pltpu.VMEM((group, part), BF16),
         in_specs=[pl.BlockSpec(memory_space=pl.ANY)] * len(operands),
         out_specs=pl.BlockSpec(memory_space=pltpu.VMEM),
         scratch_shapes=scratch,

time: 34 us -> 30.4 us (0.89)
  Pallas kernels: 32.5 us -> 29.6 us
  local copies, waits for them, and re-layouts: 1.3 us -> 0.6 us
    pallas_call x1, Pallas kernels: 32.5 us -> 29.6 us  [body(): pl.pallas_call(functools.partial(kernel, n_ep, n_tp, head_dim), out_shape...]
    unnamed x1, local copies, waits for them, and re-layouts: 1.3 us -> 0.6 us
where the time goes in v2:
time: 30.4 us; the launch traced here: 30.2 us
  Pallas kernels  29.6 us (97%)
  local copies, waits for them, and re-layouts  0.6 us (2%)
    pallas_call x1, Pallas kernels, body(): pl.pallas_call(functools.partial(kernel, n_ep, n_tp, head_dim), out_shape...  29.6 us

profile of v2, /device:TPU:0, one launch (start us, length us, event | category | flops | bytes accessed | tf_op | source)
XLA Modules:
  0.0 30.2 jit_solution(10816498759274344463)
XLA Ops:
  0.0 29.6 %shard_map.163 = bf16[8,512]{1,0:T(8,128)(2,1)S(1)} custom-call(bf16[4,1024]{1,0:T(4,128)(2,1)} %tokens_h.1, s32[8]{0:T(128)} %lengths_h.1, bf16[4,1024,128]{2,1,0:T(8,128)(2,1)} %kc_h.1, bf16[4,1024,128]{2,1,0:T(8,128)(2,1)} %vc_h.1, bf16[1024,256]{1,0:T(8,128)(2,1)} %qw_h.1, bf16[1024,128]{1,0:T(8,128)(2,1)} %kw_h.1, bf16[1024,128]{1,0:T(8,128)(2,1)} %vw_h.1, ...), custom_call_target="tpu_custom_call" | custom-call | tf_op jit(solution)/shard_map/pallas_call | solution.py:435
  29.6 0.6 %copy.19 = bf16[8,512]{1,0:T(8,128)(2,1)} copy(bf16[8,512]{1,0:T(8,128)(2,1)S(1)} %shard_map.163) | data formatting | bytes 16384

commit v3 on v2

--- a/solution.py
+++ b/solution.py
@@ -164,7 +164,7 @@
     new_value = jnp.dot(mine, vw[...], preferred_element_type=F32).astype(BF16).astype(F32)
 
     l_qw.wait()
-    for k in range(1, min(4, bits)):
+    for k in range(1, min(3, bits)):
         spread(k)
     for copy in tok_copies:
         copy.wait_recv()
@@ -178,9 +178,8 @@
             qsend[s, :, cut] = turned[s * own:(s + 1) * own, :].astype(BF16)
     q_copies = swap(qrecv, q_s, q_r, qsend)
     qrecv[t] = qsend[t]
-    for k in range(4, bits):
+    for k in range(3, min(4, bits)):
         spread(k)
-    repeat(n_ep - 1, send_w)
 
     l_lam.wait()
     l_hg.wait()
@@ -229,6 +228,9 @@
             piece = jnp.where(row_o == b, outs[b][h:h + 1, :], piece)
         att[t, :, h * LANES:(h + 1) * LANES] = piece.astype(BF16)
     att_copies = swap(att, att_s, att_r)
+    for k in range(4, bits):
+        spread(k)
+    repeat(n_ep - 1, send_w)
 
     l_ow.wait()
     l_g1.wait()

time: 30.4 us -> 30.1 us (level)
  no operation moved by 1% of the time
where the time goes in v3:
time: 30.1 us; the launch traced here: 30 us
  Pallas kernels  29.4 us (98%)
  local copies, waits for them, and re-layouts  0.6 us (2%)
    pallas_call x1, Pallas kernels, body(): pl.pallas_call(functools.partial(kernel, n_ep, n_tp, head_dim), out_shape...  29.4 us

profile of v3, /device:TPU:0, one launch (start us, length us, event | category | flops | bytes accessed | tf_op | source)
XLA Modules:
  0.0 30.0 jit_solution(9625602944117956605)
XLA Ops:
  0.0 29.4 %shard_map.163 = bf16[8,512]{1,0:T(8,128)(2,1)S(1)} custom-call(bf16[4,1024]{1,0:T(4,128)(2,1)} %tokens_h.1, s32[8]{0:T(128)} %lengths_h.1, bf16[4,1024,128]{2,1,0:T(8,128)(2,1)} %kc_h.1, bf16[4,1024,128]{2,1,0:T(8,128)(2,1)} %vc_h.1, bf16[1024,256]{1,0:T(8,128)(2,1)} %qw_h.1, bf16[1024,128]{1,0:T(8,128)(2,1)} %kw_h.1, bf16[1024,128]{1,0:T(8,128)(2,1)} %vw_h.1, ...), custom_call_target="tpu_custom_call" | custom-call | tf_op jit(solution)/shard_map/pallas_call | solution.py:437
  29.4 0.6 %copy.19 = bf16[8,512]{1,0:T(8,128)(2,1)} copy(bf16[8,512]{1,0:T(8,128)(2,1)S(1)} %shard_map.163) | data formatting | bytes 16384
